TPU v7x, 32 devices: a whole 2x2x4 slice. The times are simulated.
32 devices in a mesh: sp: 8 (over z, y), tp: 4 (over x, core).
Axes of the slice: x: 2, y: 2, z: 4, core: 2. Of those that a mesh axis runs over, the one named last changes fastest.
Arguments:
- latent: bfloat16 [2048, 2048], P('sp'), may hold values from -6 to 6
- context: bfloat16 [1024, 2048], P('sp'), may hold values from -6 to 6
- condition: bfloat16 [2048], replicated, may hold values from -6 to 6
- context_condition: bfloat16 [2048], replicated, may hold values from -6 to 6
- gain_pre: float32 [2048], replicated, may hold values from 0.1 to 1.9
- gain_post: float32 [2048], replicated, may hold values from 0.1 to 1.9
- w_shift: bfloat16 [2048, 2048], P('sp', 'tp'), may hold values from -0.125 to 0.125
- w_scale: bfloat16 [2048, 2048], P('sp', 'tp'), may hold values from -0.125 to 0.125
- w_gate: bfloat16 [2048, 2048], P('sp', 'tp'), may hold values from -0.125 to 0.125
- w_query: bfloat16 [2048, 2048], P(None, 'tp'), may hold values from -0.13258252 to 0.13258252
- w_key: bfloat16 [2048, 2048], P(None, 'tp'), may hold values from -6.629126 to 6.629126
- w_value: bfloat16 [2048, 2048], P(None, 'tp'), may hold values from -0.125 to 0.125
- w_silu: bfloat16 [2048, 2048], P(None, 'tp'), may hold values from -0.125 to 0.125
- offset_bias: float32 [32, 15, 31], P('tp'), may hold values from 1.5 to 3.5
- w_out: bfloat16 [2048, 2048], P('tp'), may hold values from -0.125 to 0.125
Outputs:
- updated: bfloat16 [2048, 2048], P(('sp', 'tp'))
All inputs are finite; a program needn't handle non-finite values.
Results may differ from a plain program's by a relative error of at most 0.01.
Values may be sent and summed in bfloat16 or wider, within the bound.
A program may use at most 64 MiB of HBM per device.

v0:
```python
import functools

import jax
import jax.numpy as jnp
from jax import lax
from jax.experimental import pallas as pl
from jax.experimental.pallas import tpu as pltpu
from jax.sharding import PartitionSpec as P

GRID_W = 64
WIN_ROWS = 8
WIN_COLS = 16
EPSILON = 1e-06
MASKED = -1e30
F32 = jnp.float32
BF16 = jnp.bfloat16
TILE = 512
PIECES = 4


def remote(src, dst, send, recv, where):
    return pltpu.make_async_remote_copy(
        src_ref=src,
        dst_ref=dst,
        send_sem=send,
        recv_sem=recv,
        device_id=where,
        device_id_type=pl.DeviceIdType.MESH,
    )


def dot(a, b):
    return jnp.dot(a, b, preferred_element_type=F32)


def dot_t(a, b):
    return lax.dot_general(a, b, (((1,), (1,)), ((), ())), preferred_element_type=F32)


def kernel(
    S,
    T,
    active,
    gain_pre,
    gain_post,
    table_rows,
    latent_hbm,
    context_hbm,
    wsh_hbm,
    wsc_hbm,
    wga_hbm,
    wq_hbm,
    wk_hbm,
    wv_hbm,
    ws_hbm,
    wo_hbm,
    out,
    lat,
    ctx,
    wmod,
    wall,
    wo,
    part,
    modbuf,
    modfull,
    modrow,
    hid,
    qg,
    kv,
    ckv,
    table,
    gated,
    prod,
    pair,
    mate,
    terms,
    load_sem,
    a_send,
    a_recv,
    b_send,
    b_recv,
    y_send,
    y_recv,
    z_send,
    z_recv,
    x_send,
    x_recv,
    d_send,
    d_recv,
    h_send,
    h_recv,
    m_send,
    m_recv,
    r_send,
    r_recv,
):
    s = lax.axis_index("sp")
    t = lax.axis_index("tp")
    width = lat.shape[1]
    tokens = lat.shape[0] // 3
    n_ctx = ctx.shape[0] // S
    cols = wo.shape[0]
    heads = table.shape[0]
    rows = tokens // GRID_W
    X, Y, Z = layout_of(S, T)
    z = s // Y
    y = s % Y
    xi = t // 2
    core = t % 2
    partner = {"tp": t + 1 - 2 * core}
    half_width = width // 2
    slice_width = width // T
    own_lat = pl.ds(tokens, tokens)

    def ctx_rows(b):
        return pl.ds(pl.multiple_of(b * n_ctx, n_ctx), n_ctx)

    def ctx_slice(b, j):
        return ctx.at[ctx_rows(b), pl.ds(pl.multiple_of(j * slice_width, slice_width), slice_width)]

    loads = []
    for i, (src, dst) in enumerate(
        [
            (context_hbm, ctx.at[ctx_rows(s)]),
            (wsh_hbm, wmod.at[0]),
            (wsc_hbm, wmod.at[1]),
            (wga_hbm, wmod.at[2]),
            (latent_hbm, lat.at[own_lat]),
            (wk_hbm, wall.at[:, pl.ds(0, cols)]),
            (wv_hbm, wall.at[:, pl.ds(cols, cols)]),
            (wq_hbm, wall.at[:, pl.ds(2 * cols, cols)]),
            (ws_hbm, wall.at[:, pl.ds(3 * cols, cols)]),
            (wo_hbm, wo),
        ]
    ):
        copy = pltpu.make_async_copy(src, dst, load_sem.at[i])
        copy.start()
        loads.append(copy)

    barrier = pltpu.get_barrier_semaphore()
    for d in range(1, S):
        pl.semaphore_signal(
            barrier, inc=1, device_id={"sp": lax.rem(s + d, S)}, device_id_type=pl.DeviceIdType.MESH
        )
    for d in range(1, T):
        pl.semaphore_signal(
            barrier, inc=1, device_id={"tp": lax.rem(t + d, T)}, device_id_type=pl.DeviceIdType.MESH
        )

    pending = []

    def send(cond, copy):
        pending.append((cond, copy))
        if cond is None:
            copy.start()
        else:

            @pl.when(cond)
            def _():
                copy.start()

    def arrive(cond, copy):
        if cond is None:
            copy.wait_recv()
        else:

            @pl.when(cond)
            def _():
                copy.wait_recv()

    part[...] = jnp.zeros_like(part)
    loads[0].wait()
    pl.semaphore_wait(barrier, S - 1 + T - 1)

    for d in range(1, Y):
        send(
            None,
            remote(
                ctx_slice(s, t),
                ctx_slice(s, t),
                y_send.at[d - 1],
                y_recv.at[d - 1],
                {"sp": z * Y + lax.rem(y + d, Y)},
            ),
        )

    def chain(way, k, u):
        at = z - k if way == 0 else z + k
        have = ((at >= 0) & (z < Z - 1)) if way == 0 else ((at <= Z - 1) & (z > 0))
        target = lax.rem(s + Y, S) if way == 0 else lax.rem(s + S - Y, S)
        b = ctx_slice(at * Y + lax.rem(y + u, Y), t)
        return have, remote(b, b, z_send.at[way, k, u], z_recv.at[way, k, u], {"sp": target})

    for way in range(2):
        if Z > 1:
            send(*chain(way, 0, 0))

    for i in range(3):
        loads[1 + i].wait()
        part[2 * i : 2 * i + 2, :] = dot(active[...], wmod[i])[0:2]

    a_copies = []
    for d in range(1, S):
        copy = remote(
            part, modbuf.at[s], a_send.at[d - 1], a_recv.at[d - 1], {"sp": lax.rem(s + d, S)}
        )
        copy.start()
        a_copies.append(copy)

    loads[4].wait()

    piece = half_width // PIECES

    def lat_part(where, side, p):
        return lat.at[
            pl.ds(where * tokens, tokens),
            pl.ds(pl.multiple_of(side * half_width + p * piece, piece), piece),
        ]

    def to_next(p):
        return remote(
            lat_part(1, core, p),
            lat_part(0, core, p),
            h_send.at[0, p],
            h_recv.at[0, p],
            {"sp": lax.rem(s + 1, S)},
        )

    def to_prev(p):
        return remote(
            lat_part(1, core, p),
            lat_part(2, core, p),
            h_send.at[1, p],
            h_recv.at[1, p],
            {"sp": lax.rem(s + S - 1, S)},
        )

    def halo_start(p):
        send(s < S - 1, to_next(p))
        send(s > 0, to_prev(p))

    halo_start(0)

    def units_of(k):
        if k < 0:
            return [(d - 1, z * Y + lax.rem(y + Y - d, Y), None) for d in range(1, Y)]
        units = []
        for way in range(2):
            at = z - 1 - k if way == 0 else z + 1 + k
            have = at >= 0 if way == 0 else at <= Z - 1
            for u in range(Y):
                units.append((Y - 1 + (k * 2 + way) * Y + u, at * Y + lax.rem(y + u, Y), have))
        return units

    def share(unit):
        n, b, have = unit
        mine = ctx_slice(b, t)
        for d in range(1, X):
            send(
                have,
                remote(
                    mine,
                    mine,
                    x_send.at[n * (X - 1) + d - 1] if X > 1 else None,
                    x_recv.at[n * (X - 1) + d - 1] if X > 1 else None,
                    {"tp": lax.rem(xi + d, X) * 2 + core},
                ),
            )
        send(have, remote(mine, mine, d_send.at[n * X], d_recv.at[n * X], partner))

    def own_arrive(k):
        for n, b, have in units_of(k):
            ref = ctx_slice(b, t)
            if k < 0:
                arrive(None, remote(ref, ref, y_send.at[n], y_recv.at[n], partner))
                u = Y - 1 - n
                if Z > 1:
                    send(*chain(0, 0, u))
                    send(*chain(1, 0, u))
            else:
                way, u = ((n - (Y - 1)) // Y) % 2, (n - (Y - 1)) % Y
                arrive(
                    have,
                    remote(ref, ref, z_send.at[way, k, u], z_recv.at[way, k, u], partner),
                )
                if k + 1 < Z - 1:
                    send(*chain(way, k + 1, u))
            share((n, b, have))

    def x_arrive(k):
        for n, b, have in units_of(k):
            for d in range(1, X):
                ref = ctx_slice(b, lax.rem(xi + X - d, X) * 2 + core)
                at = n * (X - 1) + d - 1
                arrive(have, remote(ref, ref, x_send.at[at], x_recv.at[at], partner))
                send(
                    have, remote(ref, ref, d_send.at[n * X + d], d_recv.at[n * X + d], partner)
                )

    def mate_arrive(k):
        for n, b, have in units_of(k):
            for d in range(X):
                ref = ctx_slice(b, lax.rem(xi + X - d, X) * 2 + 1 - core)
                arrive(have, remote(ref, ref, d_send.at[n * X + d], d_recv.at[n * X + d], partner))

    def hidden(src, first, count, kind):
        step = 32

        @pl.loop(0, count // step, unroll=min(4, count // step))
        def _(i):
            at = pl.ds(pl.multiple_of(first + i * step, step), step)
            v = src[at, :].astype(F32)
            inv = lax.rsqrt(jnp.mean(v * v, axis=-1, keepdims=True) + EPSILON)
            v = v * inv * modrow[2 + kind : 3 + kind, :] + modrow[kind : kind + 1, :]
            hid[pl.ds(pl.multiple_of(i * step, step), step), :] = v.astype(BF16)

    def project(count, dst, first, tiles, start):
        @pl.loop(0, tiles)
        def _(i):
            at = pl.ds(pl.multiple_of(i * TILE, TILE), TILE)
            wat = pl.ds(pl.multiple_of(start + i * TILE, TILE), TILE)
            dst[pl.ds(first, count), at] = dot(hid[0:count, :], wall[:, wat]).astype(BF16)

    def ctx_project(at):
        count = Y * n_ctx
        first = pl.multiple_of(at * count, count)
        hidden(ctx, first, count, 1)
        project(count, ckv, first, 2 * cols // TILE, 0)

    def process(k):
        mate_arrive(k)
        if k < 0:
            ctx_project(z)
        else:

            @pl.when(z - 1 - k >= 0)
            def _():
                ctx_project(z - 1 - k)

            @pl.when(z + 1 + k <= Z - 1)
            def _():
                ctx_project(z + 1 + k)

    own_arrive(-1)
    halo_start(1)

    lane = lax.broadcasted_iota(jnp.int32, (GRID_W, 2 * GRID_W), 1) % GRID_W
    row = lax.broadcasted_iota(jnp.int32, (GRID_W, 2 * GRID_W), 0)
    first = jnp.clip(row - WIN_COLS // 2, 0, GRID_W - WIN_COLS)
    inside = (lane >= first) & (lane < first + WIN_COLS)
    pairs = table.shape[1]

    @pl.loop(0, heads)
    def _(h):
        for p in range(pairs):
            line = jnp.broadcast_to(table_rows[h, p : p + 1, :], (GRID_W, 2 * GRID_W))
            rolled = pltpu.roll(
                line, 2 * GRID_W - (WIN_COLS - 1), 1, stride=1, stride_axis=0
            )
            table[h, p] = jnp.where(inside, rolled, MASKED)

    modbuf[s] = part[...]
    for copy in a_copies:
        copy.wait()
    modfull[t] = jnp.sum(modbuf[...], axis=0)
    b_copies = []
    for d in range(1, T):
        copy = remote(
            modfull.at[t],
            modfull.at[t],
            b_send.at[d - 1],
            b_recv.at[d - 1],
            {"tp": lax.rem(t + d, T)},
        )
        copy.start()
        b_copies.append(copy)

    if Z > 1:
        own_arrive(0)
    halo_start(2)
    x_arrive(-1)
    for copy in b_copies:
        copy.wait()
    for j in range(T):
        at = slice(j * cols, (j + 1) * cols)
        modrow[:, at] = modfull[j]
        modrow[2:4, at] = gain_pre[:, at] * (1.0 + modfull[j, 2:4])

    for i in range(5, 9):
        loads[i].wait()
    hidden(lat, tokens, tokens, 0)
    project(tokens, kv, tokens, 2 * cols // TILE, 0)
    if Z > 2:
        own_arrive(1)
    halo_start(3)
    project(tokens, qg, 0, 2 * cols // TILE, 2 * cols)

    def halo_share():
        for p in range(PIECES):
            arrive(s > 0, to_next(p))
            mine = lat_part(0, core, p)
            send(s > 0, remote(mine, mine, m_send.at[p], m_recv.at[p], partner))
            arrive(s < S - 1, to_prev(p))
            mine = lat_part(2, core, p)
            n = PIECES + p
            send(s < S - 1, remote(mine, mine, m_send.at[n], m_recv.at[n], partner))

    for k in range(1, Z - 1):
        if k > 1:
            own_arrive(k)
        x_arrive(k - 1)
        process(k - 2)
    if Z > 1:
        x_arrive(Z - 2)
        if Z > 2:
            process(Z - 3)
    halo_share()
    if Z > 1:
        process(Z - 2)
    else:
        process(-1)

    @pl.when(s > 0)
    def _():
        for p in range(PIECES):
            ref = lat_part(0, 1 - core, p)
            remote(ref, ref, m_send.at[p], m_recv.at[p], partner).wait_recv()
        hidden(lat, 0, tokens, 0)
        project(tokens, kv, 0, 2 * cols // TILE, 0)

    @pl.when(s < S - 1)
    def _():
        for p in range(PIECES):
            ref = lat_part(2, 1 - core, p)
            remote(ref, ref, m_send.at[PIECES + p], m_recv.at[PIECES + p], partner).wait_recv()
        hidden(lat, 2 * tokens, tokens, 0)
        project(tokens, kv, 2 * tokens, 2 * cols // TILE, 0)

    total_rows = rows * S
    half = lax.broadcasted_iota(jnp.int32, (tokens, 128), 1) < 64
    scale = 0.125

    @pl.loop(0, heads // 2)
    def _(hp):
        at = pl.ds(pl.multiple_of(hp * 128, 128), 128)
        vat = pl.ds(pl.multiple_of(cols + hp * 128, 128), 128)
        q2 = qg[:, at].astype(F32) * scale
        ck = ckv[:, at]
        cv = ckv[:, vat]
        outs = []
        for e in range(2):
            q = jnp.where(half if e == 0 else jnp.logical_not(half), q2, 0.0).astype(BF16)
            sc = dot_t(q, ck)
            sw = []
            bands = []
            for r in range(rows):
                g = s * rows + r
                rs = jnp.clip(g - WIN_ROWS // 2, 0, total_rows - WIN_ROWS)
                band = pl.ds(
                    pl.multiple_of((rs - s * rows + rows) * GRID_W, GRID_W), WIN_ROWS * GRID_W
                )
                bands.append(band)
                bias = jnp.concatenate(
                    [
                        table[hp * 2 + e, rs - g + WIN_ROWS - 1 + 2 * p]
                        for p in range(WIN_ROWS // 2)
                    ],
                    axis=1,
                )
                sw.append(dot_t(q[r * GRID_W : (r + 1) * GRID_W], kv[band, at]) + bias)
            sw = jnp.concatenate(sw, axis=0)
            m = jnp.maximum(
                jnp.max(sc, axis=-1, keepdims=True), jnp.max(sw, axis=-1, keepdims=True)
            )
            pc = jnp.exp(sc - m)
            pw = jnp.exp(sw - m)
            total = jnp.sum(pc, axis=-1, keepdims=True) + jnp.sum(pw, axis=-1, keepdims=True)
            pw = pw.astype(BF16)
            o = dot(pc.astype(BF16), cv)
            ow = [
                dot(pw[r * GRID_W : (r + 1) * GRID_W], kv[bands[r], vat]) for r in range(rows)
            ]
            outs.append((o + jnp.concatenate(ow, axis=0)) / total)
        o = jnp.where(half, outs[0], outs[1])
        gate = qg[:, vat].astype(F32)
        gated[:, at] = (gate / (1.0 + jnp.exp(-gate)) * o).astype(BF16)

    loads[9].wait()
    own = tokens // T
    groups = 4
    span = width // groups
    m_copies = []
    for g in range(groups):
        span_at = pl.ds(g * span, span)
        prod[:, span_at] = dot(gated[...], wo[:, span_at]).astype(BF16)
        copies = []
        for i in range(X):
            n = g * X + i
            copy = remote(
                prod.at[
                    pl.ds(pl.multiple_of((i * 2 + 1 - core) * own, own), own), span_at
                ],
                mate.at[i, :, span_at],
                m_send.at[2 * PIECES + n],
                m_recv.at[2 * PIECES + n],
                partner,
            )
            copy.start()
            copies.append(copy)
        m_copies.append(copies)
    r_copies = []
    for g in range(groups):
        span_at = pl.ds(g * span, span)
        for copy in m_copies[g]:
            copy.wait()
        copies = []
        for i in range(X):
            at = pl.ds(pl.multiple_of((i * 2 + core) * own, own), own)
            pair[i, :, span_at] = (
                prod[at, span_at].astype(F32) + mate[i, :, span_at].astype(F32)
            )
            if X > 1:
                prod[at, span_at] = pair[i, :, span_at].astype(BF16)
        for d in range(1, X):
            other = lax.rem(xi + d, X)
            n = g * (X - 1) + d - 1
            copy = remote(
                prod.at[pl.ds(pl.multiple_of((other * 2 + core) * own, own), own), span_at],
                terms.at[d - 1, :, span_at],
                r_send.at[n],
                r_recv.at[n],
                {"tp": other * 2 + core},
            )
            copy.start()
            copies.append(copy)
        r_copies.append(copies)
    for copies in r_copies:
        for copy in copies:
            copy.wait()
    total = pair[xi]
    for d in range(1, X):
        total = total + terms[d - 1].astype(F32)
    b = total.astype(BF16).astype(F32)
    inv = lax.rsqrt(jnp.mean(b * b, axis=-1, keepdims=True) + EPSILON)
    own_at = pl.ds(pl.multiple_of(tokens + t * own, own), own)
    out[...] = (
        lat[own_at, :].astype(F32) + modrow[4:5, :] * (b * inv * gain_post[...])
    ).astype(BF16)

    for cond, copy in pending:
        if cond is None:
            copy.wait_send()
        else:

            @pl.when(cond)
            def _(copy=copy):
                copy.wait_send()


def layout_of(S, T):
    X = T // 2
    Y = X if S % X == 0 else 1
    return X, Y, S // Y


def shards(
    S,
    T,
    latent,
    context,
    condition,
    context_condition,
    gain_pre,
    gain_post,
    w_shift,
    w_scale,
    w_gate,
    w_query,
    w_key,
    w_value,
    w_silu,
    offset_bias,
    w_out,
):
    in_rows, cols = w_shift.shape
    tokens, width = latent.shape
    n_ctx = context.shape[0]
    heads = offset_bias.shape[0]
    stacked = jnp.stack([condition, context_condition])
    own = lax.dynamic_slice_in_dim(stacked, lax.axis_index("sp") * in_rows, in_rows, 1)
    active = jnp.pad(jax.nn.silu(own.astype(F32)).astype(BF16), ((0, 14), (0, 0)))
    wide = jnp.pad(offset_bias, ((0, 0), (0, 0), (0, GRID_W - offset_bias.shape[2])))
    table_rows = jnp.concatenate([wide[:, :-1], wide[:, 1:]], axis=-1)
    pairs = table_rows.shape[1]
    own_rows = tokens // T
    vmem = pl.BlockSpec(memory_space=pltpu.VMEM)
    hbm = pl.BlockSpec(memory_space=pl.ANY)
    sem = pltpu.SemaphoreType.DMA
    X, Y, Z = layout_of(S, T)
    units = Y - 1 + 2 * (Z - 1) * Y
    return pl.pallas_call(
        functools.partial(kernel, S, T),
        out_shape=jax.ShapeDtypeStruct((own_rows, width), BF16),
        in_specs=[vmem] * 4 + [hbm] * 10,
        out_specs=vmem,
        scratch_shapes=[
            pltpu.VMEM((3 * tokens, width), BF16),
            pltpu.VMEM((S * n_ctx, width), BF16),
            pltpu.VMEM((3, in_rows, cols), BF16),
            pltpu.VMEM((width, 4 * cols), BF16),
            pltpu.VMEM((cols, width), BF16),
            pltpu.VMEM((8, cols), F32),
            pltpu.VMEM((S, 8, cols), F32),
            pltpu.VMEM((T, 8, cols), F32),
            pltpu.VMEM((8, width), F32),
            pltpu.VMEM((max(tokens, Y * n_ctx), width), BF16),
            pltpu.VMEM((tokens, 2 * cols), BF16),
            pltpu.VMEM((3 * tokens, 2 * cols), BF16),
            pltpu.VMEM((S * n_ctx, 2 * cols), BF16),
            pltpu.VMEM((heads, pairs, GRID_W, 2 * GRID_W), F32),
            pltpu.VMEM((tokens, cols), BF16),
            pltpu.VMEM((tokens, width), BF16),
            pltpu.VMEM((X, own_rows, width), F32),
            pltpu.VMEM((X, own_rows, width), BF16),
            pltpu.VMEM((max(X - 1, 1), own_rows, width), BF16),
            sem((10,)),
            sem((max(S - 1, 1),)),
            sem((max(S - 1, 1),)),
            sem((max(T - 1, 1),)),
            sem((max(T - 1, 1),)),
            sem((max(Y - 1, 1),)),
            sem((max(Y - 1, 1),)),
            sem((2, max(Z - 1, 1), Y)),
            sem((2, max(Z - 1, 1), Y)),
            sem((max(units * (X - 1), 1),)),
            sem((max(units * (X - 1), 1),)),
            sem((max(units * X, 1),)),
            sem((max(units * X, 1),)),
            sem((2, PIECES)),
            sem((2, PIECES)),
            sem((2 * PIECES + 4 * X,)),
            sem((2 * PIECES + 4 * X,)),
            sem((4 * max(X - 1, 1),)),
            sem((4 * max(X - 1, 1),)),
        ],
        compiler_params=pltpu.CompilerParams(
            collective_id=0, has_side_effects=True, vmem_limit_bytes=60 * 1024 * 1024
        ),
    )(
        active,
        gain_pre.reshape(1, width),
        gain_post.reshape(1, width),
        table_rows,
        latent,
        context,
        w_shift,
        w_scale,
        w_gate,
        w_query,
        w_key,
        w_value,
        w_silu,
        w_out,
    )


def solution(mesh):
    in_specs = (
        P("sp", None),
        P("sp", None),
        P(),
        P(),
        P(),
        P(),
        P("sp", "tp"),
        P("sp", "tp"),
        P("sp", "tp"),
        P(None, "tp"),
        P(None, "tp"),
        P(None, "tp"),
        P(None, "tp"),
        P("tp", None, None),
        P("tp", None),
    )
    return jax.shard_map(
        functools.partial(shards, mesh.shape["sp"], mesh.shape["tp"]),
        mesh=mesh,
        in_specs=in_specs,
        out_specs=P(("sp", "tp"), None),
        check_vma=False,
    )
```

profile of v0, /device:TPU:0, one launch (start us, length us, event | category | flops | bytes accessed | tf_op | source)
XLA Modules:
  0.0 70.8 jit_solution(14854854965709881589)
XLA Ops:
  0.0 0.7 stack.9
  0.7 0.7 stack.10
  1.4 0.1 fusion.2
  1.5 0.6 pad.8.active
  2.1 0.8 %copy.16 = f32[8,15,31]{2,1,0:T(8,128)S(1)} copy(f32[8,15,31]{2,0,1:T(8,128)} %param.28) | data formatting | bytes 29760 | tf_op args[13]
  3.0 0.7 %pad_maximum_fusion.table_rows = f32[8,14,128]{2,1,0:T(8,128)} fusion(f32[8,14,64]{2,1,0:T(8,128)S(1)} %get-tuple-element.6, f32[8,14,64]{2,1,0:T(8,128)S(1)} %get-tuple-element.5), kind=kLoop, calls=%fused_computation | loop fusion | flops 14336 | bytes 114688 | tf_op jit(solution)/shard_map/concatenate | solution.py:593
  3.7 65.4 %shard_map.145 = bf16[64,2048]{1,0:T(8,128)(2,1)} custom-call(bf16[16,256]{1,0:T(8,128)(2,1)} %pad.8.active, f32[1,2048]{1,0:T(1,128)} %bitcast.2, f32[1,2048]{1,0:T(1,128)} %bitcast.3, f32[8,14,128]{2,1,0:T(8,128)} %pad_maximum_fusion.table_rows, bf16[256,2048]{1,0:T(8,128)(2,1)} %latent_hbm.1, bf16[128,2048]{1,0:T(8,128)(2,1)} %context_hbm.1, ...), custom_call_target="tpu_custom_call" | custom-call | tf_op jit(solution)/shard_map/pallas_call | solution.py:601
  69.1 1.7 %copy.18 = bf16[64,2048]{1,0:T(8,128)(2,1)} copy(bf16[64,2048]{1,0:T(8,128)(2,1)} %shard_map.145) | data formatting | bytes 524288
  (1 shorter events, 0.0 us)
where the time goes:
time: 71.1 us; the launch traced here: 70.8 us
  Pallas kernels  65.4 us (92%)
  local copies, waits for them, and re-layouts  4.52 us (6%)
  other arithmetic  0.81 us (1%)
    pallas_call x1, Pallas kernels, shards(): pl.pallas_call(functools.partial(kernel, S, T), out_shape=jax.ShapeDtypeS...  65.4 us
    unnamed x2, local copies, waits for them, and re-layouts  2.51 us

commit v1 on v0

v1 whole, which is shorter than its diff:
```python
import functools

import jax
import jax.numpy as jnp
from jax import lax
from jax.experimental import pallas as pl
from jax.experimental.pallas import tpu as pltpu
from jax.sharding import PartitionSpec as P

GRID_W = 64
WIN_ROWS = 8
WIN_COLS = 16
EPSILON = 1e-06
MASKED = -1e30
F32 = jnp.float32
BF16 = jnp.bfloat16
TILE = 512
GROUPS = 4


def remote(src, dst, send, recv, where):
    return pltpu.make_async_remote_copy(
        src_ref=src,
        dst_ref=dst,
        send_sem=send,
        recv_sem=recv,
        device_id=where,
        device_id_type=pl.DeviceIdType.MESH,
    )


def dot(a, b):
    return jnp.dot(a, b, preferred_element_type=F32)


def dot_t(a, b):
    return lax.dot_general(a, b, (((1,), (1,)), ((), ())), preferred_element_type=F32)


def kernel(
    S,
    T,
    cond_hbm,
    ctx_cond_hbm,
    gain_pre_hbm,
    gain_post_hbm,
    bias_hbm,
    latent_hbm,
    context_hbm,
    wsh_hbm,
    wsc_hbm,
    wga_hbm,
    wq_hbm,
    wk_hbm,
    wv_hbm,
    ws_hbm,
    wo_hbm,
    out,
    cond_raw,
    ctx_cond_raw,
    active,
    gain_pre,
    gain_post,
    bias,
    lines,
    lat,
    ctx,
    wmod,
    wall,
    wo,
    part,
    modbuf,
    modfull,
    modrow,
    hid,
    kv_out,
    q_out,
    c_out,
    kv,
    queries,
    ckv,
    gate,
    table,
    att_out,
    att,
    prod,
    mate,
    own_sum,
    cross,
    terms,
    load_sem,
    a_send,
    a_recv,
    b_send,
    b_recv,
    f_send,
    f_recv,
    d_send,
    d_recv,
    kv_send,
    kv_recv,
    q_send,
    q_recv,
    c_send,
    c_recv,
    h_send,
    h_recv,
    o_send,
    o_recv,
    m_send,
    m_recv,
    r_send,
    r_recv,
):
    s = lax.axis_index("sp")
    t = lax.axis_index("tp")
    tokens, width = lat.shape
    n_ctx = hid.shape[0] - tokens
    cols = wo.shape[0]
    in_rows = wmod.shape[1]
    rows = tokens // GRID_W
    G = kv_out.shape[0]
    far = S // G
    X = T // 2
    xi = t // 2
    core = t % 2
    g = s // G
    me = s % G
    partner = {"tp": t + 1 - 2 * core}
    half_width = width // 2
    pairs = table.shape[1]

    def member(d):
        return lax.rem(me + d, G)

    def other(f):
        return lax.rem(g + f, far)

    loads = []

    def load(src, dst):
        copy = pltpu.make_async_copy(src, dst, load_sem.at[len(loads)])
        copy.start()
        loads.append(copy)

    load(cond_hbm, cond_raw)
    load(ctx_cond_hbm, ctx_cond_raw)
    load(wsh_hbm, wmod.at[0])
    load(wsc_hbm, wmod.at[1])
    load(wga_hbm, wmod.at[2])
    load(context_hbm, ctx.at[0])
    load(latent_hbm, lat)
    load(bias_hbm, bias)
    load(gain_pre_hbm, gain_pre)
    load(gain_post_hbm, gain_post)
    for j in range(G):
        load(wk_hbm.at[:, pl.ds(j * 128, 128)], wall.at[:, pl.ds(j * 256, 128)])
        load(wv_hbm.at[:, pl.ds(j * 128, 128)], wall.at[:, pl.ds(j * 256 + 128, 128)])
    load(wq_hbm, wall.at[:, pl.ds(2 * cols, cols)])
    load(ws_hbm, wall.at[:, pl.ds(3 * cols, cols)])
    load(wo_hbm, wo)

    barrier = pltpu.get_barrier_semaphore()
    for d in range(1, S):
        pl.semaphore_signal(
            barrier, inc=1, device_id={"sp": lax.rem(s + d, S)}, device_id_type=pl.DeviceIdType.MESH
        )
    for d in range(1, T):
        pl.semaphore_signal(
            barrier, inc=1, device_id={"tp": lax.rem(t + d, T)}, device_id_type=pl.DeviceIdType.MESH
        )

    pending = []

    def send(copy, cond=None):
        pending.append((cond, copy))
        if cond is None:
            copy.start()
        else:

            @pl.when(cond)
            def _():
                copy.start()

    part[...] = jnp.zeros_like(part)
    loads[0].wait()
    loads[1].wait()
    which = lax.broadcasted_iota(jnp.int32, (16, width), 0)
    active[...] = jnp.where(
        which == 0,
        cond_raw[...].astype(F32).reshape(1, width),
        jnp.where(which == 1, ctx_cond_raw[...].astype(F32).reshape(1, width), 0.0),
    )
    if in_rows % 128 == 0:
        own_cond = active[:, pl.ds(pl.multiple_of(s * in_rows, in_rows), in_rows)]
    else:
        shift = lax.rem(width - s * in_rows, width)
        own_cond = pltpu.roll(active[...], shift, 1)[:, 0:in_rows]
    own_active = (own_cond / (1.0 + jnp.exp(-own_cond))).astype(BF16)
    for i in range(3):
        loads[2 + i].wait()
        part[2 * i : 2 * i + 2, :] = dot(own_active, wmod[i])[0:2]
    loads[5].wait()
    pl.semaphore_wait(barrier, S - 1 + T - 1)

    a_copies = []
    for d in range(1, S):
        copy = remote(
            part, modbuf.at[s], a_send.at[d - 1], a_recv.at[d - 1], {"sp": lax.rem(s + d, S)}
        )
        copy.start()
        a_copies.append(copy)

    def half_of(f, c):
        return ctx.at[f, :, pl.ds(pl.multiple_of(c * half_width, half_width), half_width)]

    for f in range(1, far):
        send(
            remote(
                half_of(0, core),
                half_of(far - f, core),
                f_send.at[far - f - 1],
                f_recv.at[far - f - 1],
                {"sp": other(f) * G + me},
            )
        )

    lane = lax.broadcasted_iota(jnp.int32, (GRID_W, 2 * GRID_W), 1) % GRID_W
    row = lax.broadcasted_iota(jnp.int32, (GRID_W, 2 * GRID_W), 0)
    first = jnp.clip(row - WIN_COLS // 2, 0, GRID_W - WIN_COLS)
    inside = (lane >= first) & (lane < first + WIN_COLS)
    loads[7].wait()
    blank = jnp.zeros((bias.shape[1], GRID_W - bias.shape[2]), F32)
    for p in range(pairs):
        lines[p] = jnp.concatenate([bias[p], blank, bias[p + 1], blank], axis=1)
    for e in range(2):
        for p in range(pairs):
            line = jnp.broadcast_to(lines[p, pl.ds(2 * me + e, 1), :], (GRID_W, 2 * GRID_W))
            rolled = pltpu.roll(line, 2 * GRID_W - (WIN_COLS - 1), 1, stride=1, stride_axis=0)
            table[e, p] = jnp.where(inside, rolled, MASKED)

    modbuf[s] = part[...]
    for copy in a_copies:
        copy.wait()
    modfull[t] = jnp.sum(modbuf[...], axis=0)
    b_copies = []
    for d in range(1, T):
        copy = remote(
            modfull.at[t],
            modfull.at[t],
            b_send.at[d - 1],
            b_recv.at[d - 1],
            {"tp": lax.rem(t + d, T)},
        )
        copy.start()
        b_copies.append(copy)
    for i in range(6, len(loads)):
        if i != 7:
            loads[i].wait()
    for copy in b_copies:
        copy.wait()
    for j in range(T):
        at = slice(j * cols, (j + 1) * cols)
        modrow[:, at] = modfull[j]
        modrow[2:4, at] = gain_pre[:, at] * (1.0 + modfull[j, 2:4])

    def hidden(src, dst, count, kind):
        step = 32

        @pl.loop(0, count // step, unroll=min(4, count // step))
        def _(i):
            at = pl.ds(pl.multiple_of(i * step, step), step)
            v = src[at, :].astype(F32)
            inv = lax.rsqrt(jnp.mean(v * v, axis=-1, keepdims=True) + EPSILON)
            v = v * inv * modrow[2 + kind : 3 + kind, :] + modrow[kind : kind + 1, :]
            dst[at, :] = v.astype(BF16)

    hid_lat = hid.at[pl.ds(0, tokens)]
    hid_ctx = hid.at[pl.ds(tokens, n_ctx)]
    before = (me == G - 1) & (g < far - 1)
    after = (me == 0) & (g > 0)
    below = pl.ds(0, (WIN_ROWS // 2 - 1) * GRID_W)

    def slot(n):
        return pl.ds(pl.multiple_of(n * tokens, tokens), tokens)

    hidden(lat, hid_lat, tokens, 0)
    for i in range(2 * cols // TILE):
        tile = dot(hid_lat[...], wall[:, i * TILE : (i + 1) * TILE]).astype(BF16)
        for k in range(TILE // 256):
            kv_out[i * (TILE // 256) + k] = tile[:, k * 256 : (k + 1) * 256]
    for d in range(1, G):
        j = member(d)
        send(
            remote(
                kv_out.at[j],
                kv.at[slot(1 + me)],
                kv_send.at[d - 1],
                kv_recv.at[d - 1],
                {"sp": g * G + j},
            )
        )
    tile = dot(hid_lat[...], wall[:, 2 * cols : 3 * cols]).astype(BF16)
    for j in range(G):
        q_out[j] = tile[:, j * 128 : (j + 1) * 128]
    for d in range(1, G):
        j = member(d)
        send(
            remote(
                q_out.at[j],
                queries.at[me],
                q_send.at[d - 1],
                q_recv.at[d - 1],
                {"sp": g * G + j},
            )
        )
    for j in range(G):
        send(
            remote(
                kv_out.at[j],
                kv.at[slot(0)],
                h_send.at[j],
                h_recv.at[0],
                {"sp": lax.rem(g + 1, far) * G + j},
            ),
            before,
        )
        send(
            remote(
                kv_out.at[j, below],
                kv.at[pl.ds((G + 1) * tokens, (WIN_ROWS // 2 - 1) * GRID_W)],
                h_send.at[G + j],
                h_recv.at[1],
                {"sp": lax.rem(g + far - 1, far) * G + j},
            ),
            after,
        )

    def ctx_slot(f, j):
        b = other(f) * G + j
        return pl.ds(pl.multiple_of(b * n_ctx, n_ctx), n_ctx)

    def ctx_project(f):
        hidden(ctx.at[f], hid_ctx, n_ctx, 1)
        for i in range(2 * cols // TILE):
            tile = dot(hid_ctx[...], wall[:, i * TILE : (i + 1) * TILE]).astype(BF16)
            for k in range(TILE // 256):
                c_out[f, i * (TILE // 256) + k] = tile[:, k * 256 : (k + 1) * 256]
        for d in range(1, G):
            j = member(d)
            n = f * (G - 1) + d - 1
            send(
                remote(
                    c_out.at[f, j],
                    ckv.at[ctx_slot(f, me)],
                    c_send.at[n],
                    c_recv.at[n],
                    {"sp": g * G + j},
                )
            )

    ctx_project(0)
    kv[slot(1 + me), :] = kv_out[me]
    queries[me] = q_out[me]
    ckv[ctx_slot(0, me), :] = c_out[0, me]
    gate[...] = dot(hid_lat[...], wall[:, 3 * cols : 4 * cols]).astype(BF16)
    for f in range(1, far):
        ref = half_of(f, core)
        remote(ref, ref, f_send.at[f - 1], f_recv.at[f - 1], partner).wait_recv()
        send(remote(ref, ref, d_send.at[f - 1], d_recv.at[f - 1], partner))
    for f in range(1, far):
        ref = half_of(f, 1 - core)
        remote(ref, ref, d_send.at[f - 1], d_recv.at[f - 1], partner).wait_recv()
        ctx_project(f)
        ckv[ctx_slot(f, me), :] = c_out[f, me]

    for d in range(1, G):
        ref = kv.at[slot(1 + me)]
        remote(ref, ref, kv_send.at[d - 1], kv_recv.at[d - 1], partner).wait_recv()

    @pl.when(g > 0)
    def _():
        ref = kv.at[slot(0)]
        remote(ref, ref, h_send.at[0], h_recv.at[0], partner).wait_recv()

    @pl.when(g < far - 1)
    def _():
        ref = kv.at[pl.ds((G + 1) * tokens, (WIN_ROWS // 2 - 1) * GRID_W)]
        remote(ref, ref, h_send.at[G], h_recv.at[1], partner).wait_recv()

    for f in range(far):
        for d in range(1, G):
            n = f * (G - 1) + d - 1
            ref = ckv.at[ctx_slot(f, lax.rem(me + G - d, G))]
            remote(ref, ref, c_send.at[n], c_recv.at[n], partner).wait_recv()
    for d in range(1, G):
        ref = queries.at[lax.rem(me + G - d, G)]
        remote(ref, ref, q_send.at[d - 1], q_recv.at[d - 1], partner).wait_recv()

    total_rows = rows * S
    band_rows = rows // X
    span = band_rows * GRID_W
    half = lax.broadcasted_iota(jnp.int32, (span, 128), 1) < 64
    scale = 0.125

    def token_rows(x):
        return pl.ds(pl.multiple_of(x * span, span), span)

    def attend(phase, x, first, last):
        @pl.loop(first, last)
        def _(d):
            b = lax.rem(me + 1 + d, G)
            q2 = queries[b, token_rows(x), :].astype(F32) * scale
            outs = []
            for e in range(2):
                q = jnp.where(half if e == 0 else jnp.logical_not(half), q2, 0.0).astype(BF16)
                sc = dot_t(q, ckv[:, 0:128])
                sw = []
                bands = []
                for r in range(band_rows):
                    row = (g * G + b) * rows + x * band_rows + r
                    rs = jnp.clip(row - WIN_ROWS // 2, 0, total_rows - WIN_ROWS)
                    band = pl.ds(
                        pl.multiple_of((rs - g * G * rows + rows) * GRID_W, GRID_W),
                        WIN_ROWS * GRID_W,
                    )
                    bands.append(band)
                    offsets = jnp.concatenate(
                        [
                            table[e, rs - row + WIN_ROWS - 1 + 2 * p]
                            for p in range(WIN_ROWS // 2)
                        ],
                        axis=1,
                    )
                    sw.append(dot_t(q[r * GRID_W : (r + 1) * GRID_W], kv[band, 0:128]) + offsets)
                sw = jnp.concatenate(sw, axis=0)
                m = jnp.maximum(
                    jnp.max(sc, axis=-1, keepdims=True), jnp.max(sw, axis=-1, keepdims=True)
                )
                pc = jnp.exp(sc - m)
                pw = jnp.exp(sw - m)
                total = jnp.sum(pc, axis=-1, keepdims=True) + jnp.sum(pw, axis=-1, keepdims=True)
                pw = pw.astype(BF16)
                o = dot(pc.astype(BF16), ckv[:, 128:256])
                ow = [
                    dot(pw[r * GRID_W : (r + 1) * GRID_W], kv[bands[r], 128:256])
                    for r in range(band_rows)
                ]
                outs.append((o + jnp.concatenate(ow, axis=0)) / total)
            att_out[b, token_rows(x), :] = jnp.where(half, outs[0], outs[1]).astype(BF16)

            @pl.when(d < G - 1)
            def _():
                give_back(phase, x, d).start()

    def give_back(phase, x, d):
        b = lax.rem(me + 1 + d, G)
        n = phase * G + d
        return remote(
            att_out.at[b, token_rows(x)],
            att.at[me, token_rows(x)],
            o_send.at[n],
            o_recv.at[n],
            {"sp": g * G + b},
        )

    own = tokens // T
    piece = width // GROUPS

    def project_out(phase, x):
        att[me, token_rows(x), :] = att_out[me, token_rows(x), :]
        for d in range(G - 1):
            give_back(phase, x, d).wait()
        for j in range(G):
            at = slice(j * 128, (j + 1) * 128)
            a = gate[token_rows(x), at].astype(F32)
            a = a / (1.0 + jnp.exp(-a)) * att[j, token_rows(x), :].astype(F32)
            gate[token_rows(x), at] = a.astype(BF16)
        copies = []
        for n in range(GROUPS):
            at = pl.ds(n * piece, piece)
            prod[phase, :, at] = dot(gate[token_rows(x), :], wo[:, at]).astype(BF16)
            copy = remote(
                prod.at[phase, pl.ds(pl.multiple_of((1 - core) * own, own), own), at],
                mate.at[phase, :, at],
                m_send.at[phase * GROUPS + n],
                m_recv.at[phase * GROUPS + n],
                partner,
            )
            copy.start()
            copies.append(copy)
        return copies

    mine = pl.ds(pl.multiple_of(core * own, own), own)

    def cross_send(phase, x, copies):
        crossing = []
        for n in range(GROUPS):
            at = pl.ds(n * piece, piece)
            copies[n].wait()
            both = prod[phase, mine, at].astype(F32) + mate[phase, :, at].astype(F32)
            cross[phase, :, at] = both.astype(BF16)
            copy = remote(
                cross.at[phase, :, at],
                terms.at[phase, :, at],
                r_send.at[phase * GROUPS + n],
                r_recv.at[phase * GROUPS + n],
                {"tp": x * 2 + core},
            )
            copy.start()
            crossing.append(copy)
        return crossing

    crossing = []
    for phase in range(X):
        x = lax.rem(xi + phase + 1, X)
        attend(phase, x, 0, G)
        copies = project_out(phase, x)
        if phase < X - 1:
            crossing.append(cross_send(phase, x, copies))
    for n in range(GROUPS):
        at = pl.ds(n * piece, piece)
        copies[n].wait()
        total = prod[X - 1, mine, at].astype(F32) + mate[X - 1, :, at].astype(F32)
        for phase in range(X - 1):
            crossing[phase][n].wait()
            total = total + terms[phase, :, at].astype(F32)
        own_sum[:, at] = total.astype(BF16).astype(F32)
    b = own_sum[...]
    inv = lax.rsqrt(jnp.mean(b * b, axis=-1, keepdims=True) + EPSILON)
    own_at = pl.ds(pl.multiple_of(t * own, own), own)
    out[...] = (
        lat[own_at, :].astype(F32) + modrow[4:5, :] * (b * inv * gain_post[...])
    ).astype(BF16)

    for cond, copy in pending:
        if cond is None:
            copy.wait_send()
        else:

            @pl.when(cond)
            def _(copy=copy):
                copy.wait_send()


def shards(
    S,
    T,
    latent,
    context,
    condition,
    context_condition,
    gain_pre,
    gain_post,
    w_shift,
    w_scale,
    w_gate,
    w_query,
    w_key,
    w_value,
    w_silu,
    offset_bias,
    w_out,
):
    in_rows, cols = w_shift.shape
    tokens, width = latent.shape
    n_ctx = context.shape[0]
    heads = offset_bias.shape[0]
    turned = jnp.transpose(offset_bias, (1, 0, 2))
    pairs = turned.shape[0] - 1
    own_rows = tokens // T
    vmem = pl.BlockSpec(memory_space=pltpu.VMEM)
    hbm = pl.BlockSpec(memory_space=pl.ANY)
    sem = pltpu.SemaphoreType.DMA
    X = T // 2
    G = heads // 2
    far = S // G
    return pl.pallas_call(
        functools.partial(kernel, S, T),
        out_shape=jax.ShapeDtypeStruct((own_rows, width), BF16),
        in_specs=[hbm] * 15,
        out_specs=vmem,
        scratch_shapes=[
            pltpu.VMEM((width,), BF16),
            pltpu.VMEM((width,), BF16),
            pltpu.VMEM((16, width), F32),
            pltpu.VMEM((1, width), F32),
            pltpu.VMEM((1, width), F32),
            pltpu.VMEM(turned.shape, F32),
            pltpu.VMEM((pairs, heads, 2 * GRID_W), F32),
            pltpu.VMEM((tokens, width), BF16),
            pltpu.VMEM((far, n_ctx, width), BF16),
            pltpu.VMEM((3, in_rows, cols), BF16),
            pltpu.VMEM((width, 4 * cols), BF16),
            pltpu.VMEM((cols, width), BF16),
            pltpu.VMEM((8, cols), F32),
            pltpu.VMEM((S, 8, cols), F32),
            pltpu.VMEM((T, 8, cols), F32),
            pltpu.VMEM((8, width), F32),
            pltpu.VMEM((tokens + n_ctx, width), BF16),
            pltpu.VMEM((G, tokens, 256), BF16),
            pltpu.VMEM((G, tokens, 128), BF16),
            pltpu.VMEM((far, G, n_ctx, 256), BF16),
            pltpu.VMEM(((G + 2) * tokens, 256), BF16),
            pltpu.VMEM((G, tokens, 128), BF16),
            pltpu.VMEM((S * n_ctx, 256), BF16),
            pltpu.VMEM((tokens, cols), BF16),
            pltpu.VMEM((2, pairs, GRID_W, 2 * GRID_W), F32),
            pltpu.VMEM((G, tokens, 128), BF16),
            pltpu.VMEM((G, tokens, 128), BF16),
            pltpu.VMEM((X, tokens // X, width), BF16),
            pltpu.VMEM((X, own_rows, width), BF16),
            pltpu.VMEM((own_rows, width), F32),
            pltpu.VMEM((max(X - 1, 1), own_rows, width), BF16),
            pltpu.VMEM((max(X - 1, 1), own_rows, width), BF16),
            sem((13 + 2 * G,)),
            sem((max(S - 1, 1),)),
            sem((max(S - 1, 1),)),
            sem((max(T - 1, 1),)),
            sem((max(T - 1, 1),)),
            sem((max(far - 1, 1),)),
            sem((max(far - 1, 1),)),
            sem((max(far - 1, 1),)),
            sem((max(far - 1, 1),)),
            sem((max(G - 1, 1),)),
            sem((max(G - 1, 1),)),
            sem((max(G - 1, 1),)),
            sem((max(G - 1, 1),)),
            sem((max(far * (G - 1), 1),)),
            sem((max(far * (G - 1), 1),)),
            sem((2 * G,)),
            sem((2,)),
            sem((X * G,)),
            sem((X * G,)),
            sem((X * GROUPS,)),
            sem((X * GROUPS,)),
            sem((max(X - 1, 1) * GROUPS,)),
            sem((max(X - 1, 1) * GROUPS,)),
        ],
        compiler_params=pltpu.CompilerParams(
            collective_id=0, has_side_effects=True, vmem_limit_bytes=60 * 1024 * 1024
        ),
    )(
        condition,
        context_condition,
        gain_pre.reshape(1, width),
        gain_post.reshape(1, width),
        turned,
        latent,
        context,
        w_shift,
        w_scale,
        w_gate,
        w_query,
        w_key,
        w_value,
        w_silu,
        w_out,
    )


def solution(mesh):
    in_specs = (
        P("sp", None),
        P("sp", None),
        P(),
        P(),
        P(),
        P(),
        P("sp", "tp"),
        P("sp", "tp"),
        P("sp", "tp"),
        P(None, "tp"),
        P(None, "tp"),
        P(None, "tp"),
        P(None, "tp"),
        P("tp", None, None),
        P("tp", None),
    )
    return jax.shard_map(
        functools.partial(shards, mesh.shape["sp"], mesh.shape["tp"]),
        mesh=mesh,
        in_specs=in_specs,
        out_specs=P(("sp", "tp"), None),
        check_vma=False,
    )
```

time: 71.1 us -> 61.1 us (0.86)
  the two profiles are of different devices: /device:TPU:0 before, /device:TPU:21 now
where the time goes in v1:
time: 61.1 us; the launch traced here: 60.9 us
  Pallas kernels  59.2 us (97%)
  local copies, waits for them, and re-layouts  1.67 us (3%)
    pallas_call x1, Pallas kernels, shards(): pl.pallas_call(functools.partial(kernel, S, T), out_shape=jax.ShapeDtypeS...  59.2 us
    unnamed x1, local copies, waits for them, and re-layouts  1.67 us

profile of v1, /device:TPU:21, one launch (start us, length us, event | category | flops | bytes accessed | tf_op | source)
XLA Modules:
  0.0 60.9 jit_solution(8693272077062415095)
XLA Ops:
  0.0 59.2 %shard_map.145 = bf16[64,2048]{1,0:T(8,128)(2,1)} custom-call(bf16[2048]{0:T(1024)(128)(2,1)} %cond_hbm.1, bf16[2048]{0:T(1024)(128)(2,1)} %ctx_cond_hbm.1, f32[1,2048]{1,0:T(1,128)} %bitcast.4, f32[1,2048]{1,0:T(1,128)} %bitcast.5, f32[15,8,31]{2,1,0:T(8,128)} %bitcast.3, bf16[256,2048]{1,0:T(8,128)(2,1)} %latent_hbm.1, bf16[128,2048]{1,0:T(8,128)(2,1)} %context_hbm.1, ...), custom_call_target="tpu_custom_call" | custom-call | tf_op jit(solution)/shard_map/pallas_call | solution.py:578
  59.3 1.7 %copy.17 = bf16[64,2048]{1,0:T(8,128)(2,1)} copy(bf16[64,2048]{1,0:T(8,128)(2,1)} %shard_map.145) | data formatting | bytes 524288

commit v2 on v1

--- a/solution.py
+++ b/solution.py
@@ -95,6 +95,8 @@
     b_recv,
     f_send,
     f_recv,
+    fx_send,
+    fx_recv,
     d_send,
     d_recv,
     kv_send,
@@ -131,7 +133,14 @@
     pairs = table.shape[1]
 
     def member(d):
+        if G & (G - 1) == 0:
+            return me + d - 2 * (me & d)
         return lax.rem(me + d, G)
+
+    def member_back(d):
+        if G & (G - 1) == 0:
+            return member(d)
+        return lax.rem(me + G - d, G)
 
     def other(f):
         return lax.rem(g + f, far)
@@ -211,19 +220,44 @@
         copy.start()
         a_copies.append(copy)
 
-    def half_of(f, c):
-        return ctx.at[f, :, pl.ds(pl.multiple_of(c * half_width, half_width), half_width)]
-
-    for f in range(1, far):
-        send(
-            remote(
-                half_of(0, core),
-                half_of(far - f, core),
-                f_send.at[far - f - 1],
-                f_recv.at[far - f - 1],
-                {"sp": other(f) * G + me},
-            )
-        )
+    quarter = width // T
+
+    def part_of(f, x, c):
+        at = pl.ds(pl.multiple_of((x * 2 + c) * quarter, quarter), quarter)
+        return ctx.at[f, :, at]
+
+    def ctx_cross():
+        for f in range(1, far):
+            ref = part_of(f, xi, core)
+            remote(ref, ref, f_send.at[f - 1], f_recv.at[f - 1], partner).wait_recv()
+            for d in range(1, X):
+                n = (f - 1) * (X - 1) + d - 1
+                send(
+                    remote(
+                        ref,
+                        ref,
+                        fx_send.at[n],
+                        fx_recv.at[n],
+                        {"tp": lax.rem(xi + d, X) * 2 + core},
+                    )
+                )
+            n = (f - 1) * X
+            send(remote(ref, ref, d_send.at[n], d_recv.at[n], partner))
+
+    def ctx_pass():
+        for f in range(1, far):
+            for d in range(1, X):
+                ref = part_of(f, lax.rem(xi + X - d, X), core)
+                n = (f - 1) * (X - 1) + d - 1
+                remote(ref, ref, fx_send.at[n], fx_recv.at[n], partner).wait_recv()
+                n = (f - 1) * X + d
+                send(remote(ref, ref, d_send.at[n], d_recv.at[n], partner))
+
+    def ctx_arrive(f):
+        for d in range(X):
+            ref = part_of(f, lax.rem(xi + X - d, X), 1 - core)
+            n = (f - 1) * X + d
+            remote(ref, ref, d_send.at[n], d_recv.at[n], partner).wait_recv()
 
     lane = lax.broadcasted_iota(jnp.int32, (GRID_W, 2 * GRID_W), 1) % GRID_W
     row = lax.broadcasted_iota(jnp.int32, (GRID_W, 2 * GRID_W), 0)
@@ -254,6 +288,16 @@
         )
         copy.start()
         b_copies.append(copy)
+    for f in range(1, far):
+        send(
+            remote(
+                part_of(0, xi, core),
+                part_of(far - f, xi, core),
+                f_send.at[far - f - 1],
+                f_recv.at[far - f - 1],
+                {"sp": other(f) * G + me},
+            )
+        )
     for i in range(6, len(loads)):
         if i != 7:
             loads[i].wait()
@@ -277,9 +321,6 @@
 
     hid_lat = hid.at[pl.ds(0, tokens)]
     hid_ctx = hid.at[pl.ds(tokens, n_ctx)]
-    before = (me == G - 1) & (g < far - 1)
-    after = (me == 0) & (g > 0)
-    below = pl.ds(0, (WIN_ROWS // 2 - 1) * GRID_W)
 
     def slot(n):
         return pl.ds(pl.multiple_of(n * tokens, tokens), tokens)
@@ -300,6 +341,7 @@
                 {"sp": g * G + j},
             )
         )
+    ctx_cross()
     tile = dot(hid_lat[...], wall[:, 2 * cols : 3 * cols]).astype(BF16)
     for j in range(G):
         q_out[j] = tile[:, j * 128 : (j + 1) * 128]
@@ -314,28 +356,6 @@
                 {"sp": g * G + j},
             )
         )
-    for j in range(G):
-        send(
-            remote(
-                kv_out.at[j],
-                kv.at[slot(0)],
-                h_send.at[j],
-                h_recv.at[0],
-                {"sp": lax.rem(g + 1, far) * G + j},
-            ),
-            before,
-        )
-        send(
-            remote(
-                kv_out.at[j, below],
-                kv.at[pl.ds((G + 1) * tokens, (WIN_ROWS // 2 - 1) * GRID_W)],
-                h_send.at[G + j],
-                h_recv.at[1],
-                {"sp": lax.rem(g + far - 1, far) * G + j},
-            ),
-            after,
-        )
-
     def ctx_slot(f, j):
         b = other(f) * G + j
         return pl.ds(pl.multiple_of(b * n_ctx, n_ctx), n_ctx)
@@ -360,23 +380,40 @@
             )
 
     ctx_project(0)
+    ctx_pass()
     kv[slot(1 + me), :] = kv_out[me]
     queries[me] = q_out[me]
     ckv[ctx_slot(0, me), :] = c_out[0, me]
     gate[...] = dot(hid_lat[...], wall[:, 3 * cols : 4 * cols]).astype(BF16)
     for f in range(1, far):
-        ref = half_of(f, core)
-        remote(ref, ref, f_send.at[f - 1], f_recv.at[f - 1], partner).wait_recv()
-        send(remote(ref, ref, d_send.at[f - 1], d_recv.at[f - 1], partner))
-    for f in range(1, far):
-        ref = half_of(f, 1 - core)
-        remote(ref, ref, d_send.at[f - 1], d_recv.at[f - 1], partner).wait_recv()
+        ctx_arrive(f)
         ctx_project(f)
         ckv[ctx_slot(f, me), :] = c_out[f, me]
 
     for d in range(1, G):
         ref = kv.at[slot(1 + me)]
         remote(ref, ref, kv_send.at[d - 1], kv_recv.at[d - 1], partner).wait_recv()
+    low = (WIN_ROWS // 2 - 1) * GRID_W
+    send(
+        remote(
+            kv.at[slot(G)],
+            kv.at[slot(0)],
+            h_send.at[0],
+            h_recv.at[0],
+            {"sp": lax.rem(s + G, S)},
+        ),
+        g < far - 1,
+    )
+    send(
+        remote(
+            kv.at[pl.ds(tokens, low)],
+            kv.at[pl.ds((G + 1) * tokens, low)],
+            h_send.at[1],
+            h_recv.at[1],
+            {"sp": lax.rem(s + S - G, S)},
+        ),
+        g > 0,
+    )
 
     @pl.when(g > 0)
     def _():
@@ -385,16 +422,16 @@
 
     @pl.when(g < far - 1)
     def _():
-        ref = kv.at[pl.ds((G + 1) * tokens, (WIN_ROWS // 2 - 1) * GRID_W)]
-        remote(ref, ref, h_send.at[G], h_recv.at[1], partner).wait_recv()
+        ref = kv.at[pl.ds((G + 1) * tokens, low)]
+        remote(ref, ref, h_send.at[1], h_recv.at[1], partner).wait_recv()
 
     for f in range(far):
         for d in range(1, G):
             n = f * (G - 1) + d - 1
-            ref = ckv.at[ctx_slot(f, lax.rem(me + G - d, G))]
+            ref = ckv.at[ctx_slot(f, member_back(d))]
             remote(ref, ref, c_send.at[n], c_recv.at[n], partner).wait_recv()
     for d in range(1, G):
-        ref = queries.at[lax.rem(me + G - d, G)]
+        ref = queries.at[member_back(d)]
         remote(ref, ref, q_send.at[d - 1], q_recv.at[d - 1], partner).wait_recv()
 
     total_rows = rows * S
@@ -512,12 +549,16 @@
         return crossing
 
     crossing = []
-    for phase in range(X):
-        x = lax.rem(xi + phase + 1, X)
-        attend(phase, x, 0, G)
-        copies = project_out(phase, x)
-        if phase < X - 1:
-            crossing.append(cross_send(phase, x, copies))
+    order = [lax.rem(xi + phase + 1, X) for phase in range(X)]
+    attend(0, order[0], 0, G)
+    for phase in range(1, X):
+        x, ahead = order[phase], order[phase - 1]
+        attend(phase, x, 0, 1)
+        copies = project_out(phase - 1, ahead)
+        attend(phase, x, 1, G - 1)
+        crossing.append(cross_send(phase - 1, ahead, copies))
+        attend(phase, x, G - 1, G)
+    copies = project_out(X - 1, order[X - 1])
     for n in range(GROUPS):
         at = pl.ds(n * piece, piece)
         copies[n].wait()
@@ -620,15 +661,17 @@
             sem((max(T - 1, 1),)),
             sem((max(far - 1, 1),)),
             sem((max(far - 1, 1),)),
-            sem((max(far - 1, 1),)),
-            sem((max(far - 1, 1),)),
+            sem((max((far - 1) * (X - 1), 1),)),
+            sem((max((far - 1) * (X - 1), 1),)),
+            sem((max((far - 1) * X, 1),)),
+            sem((max((far - 1) * X, 1),)),
             sem((max(G - 1, 1),)),
             sem((max(G - 1, 1),)),
             sem((max(G - 1, 1),)),
             sem((max(G - 1, 1),)),
             sem((max(far * (G - 1), 1),)),
             sem((max(far * (G - 1), 1),)),
-            sem((2 * G,)),
+            sem((2,)),
             sem((2,)),
             sem((X * G,)),
             sem((X * G,)),

time: 61.1 us -> 53.9 us (0.88)
  the two profiles are of different devices: /device:TPU:21 before, /device:TPU:0 now
where the time goes in v2:
time: 53.9 us; the launch traced here: 53.7 us
  Pallas kernels  52 us (96%)
  local copies, waits for them, and re-layouts  1.67 us (3%)
    pallas_call x1, Pallas kernels, shards(): pl.pallas_call(functools.partial(kernel, S, T), out_shape=jax.ShapeDtypeS...  52 us
    unnamed x1, local copies, waits for them, and re-layouts  1.67 us

profile of v2, /device:TPU:0, one launch (start us, length us, event | category | flops | bytes accessed | tf_op | source)
XLA Modules:
  0.0 53.7 jit_solution(1164110168627744971)
XLA Ops:
  0.0 52.0 %shard_map.145 = bf16[64,2048]{1,0:T(8,128)(2,1)} custom-call(bf16[2048]{0:T(1024)(128)(2,1)} %cond_hbm.1, bf16[2048]{0:T(1024)(128)(2,1)} %ctx_cond_hbm.1, f32[1,2048]{1,0:T(1,128)} %bitcast.4, f32[1,2048]{1,0:T(1,128)} %bitcast.5, f32[15,8,31]{2,1,0:T(8,128)} %bitcast.3, bf16[256,2048]{1,0:T(8,128)(2,1)} %latent_hbm.1, bf16[128,2048]{1,0:T(8,128)(2,1)} %context_hbm.1, ...), custom_call_target="tpu_custom_call" | custom-call | tf_op jit(solution)/shard_map/pallas_call | solution.py:619
  52.0 1.7 %copy.17 = bf16[64,2048]{1,0:T(8,128)(2,1)} copy(bf16[64,2048]{1,0:T(8,128)(2,1)} %shard_map.145) | data formatting | bytes 524288

commit v3 on v2

--- a/solution.py
+++ b/solution.py
@@ -16,6 +16,7 @@
 BF16 = jnp.bfloat16
 TILE = 512
 GROUPS = 4
+PIECES = 2
 
 
 def remote(src, dst, send, recv, where):
@@ -89,6 +90,7 @@
     cross,
     terms,
     load_sem,
+    wave_sem,
     a_send,
     a_recv,
     b_send,
@@ -99,6 +101,10 @@
     fx_recv,
     d_send,
     d_recv,
+    g_send,
+    g_recv,
+    gm_send,
+    gm_recv,
     kv_send,
     kv_recv,
     q_send,
@@ -116,8 +122,9 @@
 ):
     s = lax.axis_index("sp")
     t = lax.axis_index("tp")
-    tokens, width = lat.shape
-    n_ctx = hid.shape[0] - tokens
+    tokens = gate.shape[0]
+    width = lat.shape[1]
+    n_ctx = ctx.shape[1]
     cols = wo.shape[0]
     in_rows = wmod.shape[1]
     rows = tokens // GRID_W
@@ -131,6 +138,9 @@
     partner = {"tp": t + 1 - 2 * core}
     half_width = width // 2
     pairs = table.shape[1]
+    halved = grid_halved(S, T, G)
+    part_rows = tokens // 2
+    own_first = part_rows if halved else 0
 
     def member(d):
         if G & (G - 1) == 0:
@@ -152,13 +162,13 @@
         copy.start()
         loads.append(copy)
 
+    load(latent_hbm, lat.at[pl.ds(own_first, tokens)])
     load(cond_hbm, cond_raw)
     load(ctx_cond_hbm, ctx_cond_raw)
     load(wsh_hbm, wmod.at[0])
     load(wsc_hbm, wmod.at[1])
     load(wga_hbm, wmod.at[2])
     load(context_hbm, ctx.at[0])
-    load(latent_hbm, lat)
     load(bias_hbm, bias)
     load(gain_pre_hbm, gain_pre)
     load(gain_post_hbm, gain_post)
@@ -169,11 +179,27 @@
     load(ws_hbm, wall.at[:, pl.ds(3 * cols, cols)])
     load(wo_hbm, wo)
 
+    _, Y, Z = layout_of(S, T)
+    y = s % Y
+    z = s // Y
+    near = [(y < Y - 1, 1), (y > 0, S - 1), (z < Z - 1, Y), (z > 0, S - Y)]
+
+    def greet(sem):
+        for cond, step in near:
+
+            @pl.when(cond)
+            def _(step=step):
+                pl.semaphore_signal(
+                    sem,
+                    inc=1,
+                    device_id={"sp": lax.rem(s + step, S)},
+                    device_id_type=pl.DeviceIdType.MESH,
+                )
+
+    n_near = sum(jnp.where(cond, 1, 0) for cond, _ in near)
+
     barrier = pltpu.get_barrier_semaphore()
-    for d in range(1, S):
-        pl.semaphore_signal(
-            barrier, inc=1, device_id={"sp": lax.rem(s + d, S)}, device_id_type=pl.DeviceIdType.MESH
-        )
+    greet(barrier)
     for d in range(1, T):
         pl.semaphore_signal(
             barrier, inc=1, device_id={"tp": lax.rem(t + d, T)}, device_id_type=pl.DeviceIdType.MESH
@@ -191,26 +217,58 @@
             def _():
                 copy.start()
 
+    def side_rows(k):
+        return pl.ds(k * (own_first + tokens), part_rows)
+
+    def side_of(k, c):
+        return lat.at[
+            side_rows(k), pl.ds(pl.multiple_of(c * half_width, half_width), half_width)
+        ]
+
+    def side_send(p):
+        size = part_rows // PIECES
+        at = pl.ds(pl.multiple_of(core * half_width, half_width), half_width)
+        for k in range(2):
+            first = k * (own_first + tokens) + p * size
+            send(
+                remote(
+                    lat.at[pl.ds(own_first + k * part_rows + p * size, size), at],
+                    lat.at[pl.ds(first, size), at],
+                    g_send.at[k * PIECES + p],
+                    g_recv.at[k * PIECES + p],
+                    {"sp": g * G + member(k + 1)},
+                )
+            )
+
+    def modulate():
+        loads[1].wait()
+        loads[2].wait()
+        which = lax.broadcasted_iota(jnp.int32, (16, width), 0)
+        active[...] = jnp.where(
+            which == 0,
+            cond_raw[...].astype(F32).reshape(1, width),
+            jnp.where(which == 1, ctx_cond_raw[...].astype(F32).reshape(1, width), 0.0),
+        )
+        if in_rows % 128 == 0:
+            own_cond = active[:, pl.ds(pl.multiple_of(s * in_rows, in_rows), in_rows)]
+        else:
+            shift = lax.rem(width - s * in_rows, width)
+            own_cond = pltpu.roll(active[...], shift, 1)[:, 0:in_rows]
+        own_active = (own_cond / (1.0 + jnp.exp(-own_cond))).astype(BF16)
+        for i in range(3):
+            loads[3 + i].wait()
+            part[2 * i : 2 * i + 2, :] = dot(own_active, wmod[i])[0:2]
+
     part[...] = jnp.zeros_like(part)
-    loads[0].wait()
-    loads[1].wait()
-    which = lax.broadcasted_iota(jnp.int32, (16, width), 0)
-    active[...] = jnp.where(
-        which == 0,
-        cond_raw[...].astype(F32).reshape(1, width),
-        jnp.where(which == 1, ctx_cond_raw[...].astype(F32).reshape(1, width), 0.0),
-    )
-    if in_rows % 128 == 0:
-        own_cond = active[:, pl.ds(pl.multiple_of(s * in_rows, in_rows), in_rows)]
-    else:
-        shift = lax.rem(width - s * in_rows, width)
-        own_cond = pltpu.roll(active[...], shift, 1)[:, 0:in_rows]
-    own_active = (own_cond / (1.0 + jnp.exp(-own_cond))).astype(BF16)
-    for i in range(3):
-        loads[2 + i].wait()
-        part[2 * i : 2 * i + 2, :] = dot(own_active, wmod[i])[0:2]
-    loads[5].wait()
-    pl.semaphore_wait(barrier, S - 1 + T - 1)
+    modulate()
+    if halved:
+        loads[0].wait()
+    pl.semaphore_wait(barrier, n_near + T - 1)
+    if halved:
+        side_send(0)
+    for w in range(Y + Z - 3):
+        greet(wave_sem.at[w])
+        pl.semaphore_wait(wave_sem.at[w], n_near)
 
     a_copies = []
     for d in range(1, S):
@@ -259,6 +317,10 @@
             n = (f - 1) * X + d
             remote(ref, ref, d_send.at[n], d_recv.at[n], partner).wait_recv()
 
+    if halved:
+        for p in range(1, PIECES):
+            side_send(p)
+
     lane = lax.broadcasted_iota(jnp.int32, (GRID_W, 2 * GRID_W), 1) % GRID_W
     row = lax.broadcasted_iota(jnp.int32, (GRID_W, 2 * GRID_W), 0)
     first = jnp.clip(row - WIN_COLS // 2, 0, GRID_W - WIN_COLS)
@@ -288,6 +350,7 @@
         )
         copy.start()
         b_copies.append(copy)
+    loads[6].wait()
     for f in range(1, far):
         send(
             remote(
@@ -298,9 +361,20 @@
                 {"sp": other(f) * G + me},
             )
         )
-    for i in range(6, len(loads)):
-        if i != 7:
-            loads[i].wait()
+    if halved:
+        size = part_rows // PIECES
+        for k in range(2):
+            for p in range(PIECES):
+                at = pl.ds(pl.multiple_of(core * half_width, half_width), half_width)
+                ref = lat.at[pl.ds(k * (own_first + tokens) + p * size, size), at]
+                n = k * PIECES + p
+                remote(ref, ref, g_send.at[n], g_recv.at[n], partner).wait_recv()
+            ref = side_of(k, core)
+            send(remote(ref, ref, gm_send.at[k], gm_recv.at[k], partner))
+    for i in range(8, len(loads)):
+        loads[i].wait()
+    if not halved:
+        loads[0].wait()
     for copy in b_copies:
         copy.wait()
     for j in range(T):
@@ -319,43 +393,89 @@
             v = v * inv * modrow[2 + kind : 3 + kind, :] + modrow[kind : kind + 1, :]
             dst[at, :] = v.astype(BF16)
 
-    hid_lat = hid.at[pl.ds(0, tokens)]
-    hid_ctx = hid.at[pl.ds(tokens, n_ctx)]
+    own_rows = pl.ds(own_first, tokens)
+    hid_ctx = hid.at[pl.ds(lat.shape[0], n_ctx)]
 
     def slot(n):
         return pl.ds(pl.multiple_of(n * tokens, tokens), tokens)
 
-    hidden(lat, hid_lat, tokens, 0)
-    for i in range(2 * cols // TILE):
-        tile = dot(hid_lat[...], wall[:, i * TILE : (i + 1) * TILE]).astype(BF16)
-        for k in range(TILE // 256):
-            kv_out[i * (TILE // 256) + k] = tile[:, k * 256 : (k + 1) * 256]
-    for d in range(1, G):
-        j = member(d)
-        send(
-            remote(
+    def half_slot(n, k):
+        return pl.ds(pl.multiple_of(n * tokens + k * part_rows, part_rows), part_rows)
+
+    hidden(lat.at[own_rows], hid.at[own_rows], tokens, 0)
+    kv_done = []
+    q_done = []
+    if halved:
+        for k in range(2):
+            ref = side_of(k, 1 - core)
+            remote(ref, ref, gm_send.at[k], gm_recv.at[k], partner).wait_recv()
+            hidden(lat.at[side_rows(k)], hid.at[side_rows(k)], part_rows, 0)
+        sides = [
+            (member(1), pl.ds(tokens, tokens), [(me, 1), (member(2), 1)]),
+            (member(2), pl.ds(0, tokens), [(member(1), 0), (me, 0)]),
+        ]
+
+        def pair_dot(rows, j, first, size):
+            at = pl.ds(pl.multiple_of(first + j * size, size), size)
+            return dot(hid[rows, :], wall[:, at]).astype(BF16)
+
+        def spread(first, size, staged, target, send_sems, recv_sems, done):
+            for k, (j, rows, places) in enumerate(sides):
+                staged[k] = pair_dot(rows, j, first, size)
+                for n, (b, lower) in enumerate(places):
+                    i = 2 * k + n
+                    ref = target(b, lower)
+                    copy = remote(
+                        staged.at[k, pl.ds(n * part_rows, part_rows)],
+                        ref,
+                        send_sems.at[i],
+                        recv_sems.at[i],
+                        {"sp": g * G + j},
+                    )
+                    send(copy)
+                    done.append(copy)
+
+        def kv_part(b, k):
+            return kv.at[half_slot(1 + b, k)]
+
+        def q_part(b, k):
+            return queries.at[b, pl.ds(k * part_rows, part_rows)]
+
+        spread(0, 256, kv_out, kv_part, kv_send, kv_recv, kv_done)
+        ctx_cross()
+        spread(2 * cols, 128, q_out, q_part, q_send, q_recv, q_done)
+    else:
+        for i in range(2 * cols // TILE):
+            tile = dot(hid[own_rows, :], wall[:, i * TILE : (i + 1) * TILE]).astype(BF16)
+            for k in range(TILE // 256):
+                kv_out[i * (TILE // 256) + k] = tile[:, k * 256 : (k + 1) * 256]
+        for d in range(1, G):
+            j = member(d)
+            copy = remote(
                 kv_out.at[j],
                 kv.at[slot(1 + me)],
                 kv_send.at[d - 1],
                 kv_recv.at[d - 1],
                 {"sp": g * G + j},
             )
-        )
-    ctx_cross()
-    tile = dot(hid_lat[...], wall[:, 2 * cols : 3 * cols]).astype(BF16)
-    for j in range(G):
-        q_out[j] = tile[:, j * 128 : (j + 1) * 128]
-    for d in range(1, G):
-        j = member(d)
-        send(
-            remote(
+            send(copy)
+            kv_done.append(copy)
+        ctx_cross()
+        tile = dot(hid[own_rows, :], wall[:, 2 * cols : 3 * cols]).astype(BF16)
+        for j in range(G):
+            q_out[j] = tile[:, j * 128 : (j + 1) * 128]
+        for d in range(1, G):
+            j = member(d)
+            copy = remote(
                 q_out.at[j],
                 queries.at[me],
                 q_send.at[d - 1],
                 q_recv.at[d - 1],
                 {"sp": g * G + j},
             )
-        )
+            send(copy)
+            q_done.append(copy)
+
     def ctx_slot(f, j):
         b = other(f) * G + j
         return pl.ds(pl.multiple_of(b * n_ctx, n_ctx), n_ctx)
@@ -381,18 +501,27 @@
 
     ctx_project(0)
     ctx_pass()
-    kv[slot(1 + me), :] = kv_out[me]
-    queries[me] = q_out[me]
+    if halved:
+        tile = pair_dot(pl.ds(0, 2 * tokens), me, 0, 256)
+        kv[half_slot(1 + member(1), 0), :] = tile[0:part_rows]
+        kv[slot(1 + me), :] = tile[part_rows : part_rows + tokens]
+        kv[half_slot(1 + member(2), 1), :] = tile[part_rows + tokens :]
+        tile = pair_dot(pl.ds(0, 2 * tokens), me, 2 * cols, 128)
+        queries[member(1), 0:part_rows, :] = tile[0:part_rows]
+        queries[me] = tile[part_rows : part_rows + tokens]
+        queries[member(2), part_rows:tokens, :] = tile[part_rows + tokens :]
+    else:
+        kv[slot(1 + me), :] = kv_out[me]
+        queries[me] = q_out[me]
     ckv[ctx_slot(0, me), :] = c_out[0, me]
-    gate[...] = dot(hid_lat[...], wall[:, 3 * cols : 4 * cols]).astype(BF16)
+    gate[...] = dot(hid[own_rows, :], wall[:, 3 * cols : 4 * cols]).astype(BF16)
     for f in range(1, far):
         ctx_arrive(f)
         ctx_project(f)
         ckv[ctx_slot(f, me), :] = c_out[f, me]
 
-    for d in range(1, G):
-        ref = kv.at[slot(1 + me)]
-        remote(ref, ref, kv_send.at[d - 1], kv_recv.at[d - 1], partner).wait_recv()
+    for copy in kv_done:
+        copy.wait_recv()
     low = (WIN_ROWS // 2 - 1) * GRID_W
     send(
         remote(
@@ -430,9 +559,8 @@
             n = f * (G - 1) + d - 1
             ref = ckv.at[ctx_slot(f, member_back(d))]
             remote(ref, ref, c_send.at[n], c_recv.at[n], partner).wait_recv()
-    for d in range(1, G):
-        ref = queries.at[member_back(d)]
-        remote(ref, ref, q_send.at[d - 1], q_recv.at[d - 1], partner).wait_recv()
+    for copy in q_done:
+        copy.wait_recv()
 
     total_rows = rows * S
     band_rows = rows // X
@@ -569,7 +697,7 @@
         own_sum[:, at] = total.astype(BF16).astype(F32)
     b = own_sum[...]
     inv = lax.rsqrt(jnp.mean(b * b, axis=-1, keepdims=True) + EPSILON)
-    own_at = pl.ds(pl.multiple_of(t * own, own), own)
+    own_at = pl.ds(pl.multiple_of(own_first + t * own, own), own)
     out[...] = (
         lat[own_at, :].astype(F32) + modrow[4:5, :] * (b * inv * gain_post[...])
     ).astype(BF16)
@@ -582,6 +710,16 @@
             @pl.when(cond)
             def _(copy=copy):
                 copy.wait_send()
+
+
+def layout_of(S, T):
+    X = T // 2
+    Y = X if S % X == 0 else 1
+    return X, Y, S // Y
+
+
+def grid_halved(S, T, G):
+    return G == 4 and layout_of(S, T)[1] == 2
 
 
 def shards(
@@ -616,6 +754,8 @@
     X = T // 2
     G = heads // 2
     far = S // G
+    held = 2 * tokens if grid_halved(S, T, G) else tokens
+    _, Y, Z = layout_of(S, T)
     return pl.pallas_call(
         functools.partial(kernel, S, T),
         out_shape=jax.ShapeDtypeStruct((own_rows, width), BF16),
@@ -629,7 +769,7 @@
             pltpu.VMEM((1, width), F32),
             pltpu.VMEM(turned.shape, F32),
             pltpu.VMEM((pairs, heads, 2 * GRID_W), F32),
-            pltpu.VMEM((tokens, width), BF16),
+            pltpu.VMEM((held, width), BF16),
             pltpu.VMEM((far, n_ctx, width), BF16),
             pltpu.VMEM((3, in_rows, cols), BF16),
             pltpu.VMEM((width, 4 * cols), BF16),
@@ -638,7 +778,7 @@
             pltpu.VMEM((S, 8, cols), F32),
             pltpu.VMEM((T, 8, cols), F32),
             pltpu.VMEM((8, width), F32),
-            pltpu.VMEM((tokens + n_ctx, width), BF16),
+            pltpu.VMEM((held + n_ctx, width), BF16),
             pltpu.VMEM((G, tokens, 256), BF16),
             pltpu.VMEM((G, tokens, 128), BF16),
             pltpu.VMEM((far, G, n_ctx, 256), BF16),
@@ -655,6 +795,7 @@
             pltpu.VMEM((max(X - 1, 1), own_rows, width), BF16),
             pltpu.VMEM((max(X - 1, 1), own_rows, width), BF16),
             sem((13 + 2 * G,)),
+            pltpu.SemaphoreType.REGULAR((max(Y + Z - 3, 1),)),
             sem((max(S - 1, 1),)),
             sem((max(S - 1, 1),)),
             sem((max(T - 1, 1),)),
@@ -665,10 +806,14 @@
             sem((max((far - 1) * (X - 1), 1),)),
             sem((max((far - 1) * X, 1),)),
             sem((max((far - 1) * X, 1),)),
-            sem((max(G - 1, 1),)),
-            sem((max(G - 1, 1),)),
-            sem((max(G - 1, 1),)),
-            sem((max(G - 1, 1),)),
+            sem((2 * PIECES,)),
+            sem((2 * PIECES,)),
+            sem((2,)),
+            sem((2,)),
+            sem((G,)),
+            sem((G,)),
+            sem((G,)),
+            sem((G,)),
             sem((max(far * (G - 1), 1),)),
             sem((max(far * (G - 1), 1),)),
             sem((2,)),

time: 53.9 us -> 53 us (0.983)
  Pallas kernels: 52 us -> 51.1 us
    pallas_call x1, Pallas kernels: 52 us -> 51.1 us  [shards(): pl.pallas_call(functools.partial(kernel, S, T), out_shape=jax.ShapeDtypeS...]
where the time goes in v3:
time: 53 us; the launch traced here: 52.8 us
  Pallas kernels  51.1 us (96%)
  local copies, waits for them, and re-layouts  1.67 us (3%)
    pallas_call x1, Pallas kernels, shards(): pl.pallas_call(functools.partial(kernel, S, T), out_shape=jax.ShapeDtypeS...  51.1 us
    unnamed x1, local copies, waits for them, and re-layouts  1.67 us

profile of v3, /device:TPU:0, one launch (start us, length us, event | category | flops | bytes accessed | tf_op | source)
XLA Modules:
  0.0 52.8 jit_solution(1480616062384183860)
XLA Ops:
  0.0 51.1 %shard_map.145 = bf16[64,2048]{1,0:T(8,128)(2,1)} custom-call(bf16[2048]{0:T(1024)(128)(2,1)} %cond_hbm.1, bf16[2048]{0:T(1024)(128)(2,1)} %ctx_cond_hbm.1, f32[1,2048]{1,0:T(1,128)} %bitcast.4, f32[1,2048]{1,0:T(1,128)} %bitcast.5, f32[15,8,31]{2,1,0:T(8,128)} %bitcast.3, bf16[256,2048]{1,0:T(8,128)(2,1)} %latent_hbm.1, bf16[128,2048]{1,0:T(8,128)(2,1)} %context_hbm.1, ...), custom_call_target="tpu_custom_call" | custom-call | tf_op jit(solution)/shard_map/pallas_call | solution.py:759
  51.2 1.7 %copy.17 = bf16[64,2048]{1,0:T(8,128)(2,1)} copy(bf16[64,2048]{1,0:T(8,128)(2,1)} %shard_map.145) | data formatting | bytes 524288

commit v4 on v3

--- a/solution.py
+++ b/solution.py
@@ -15,7 +15,7 @@
 F32 = jnp.float32
 BF16 = jnp.bfloat16
 TILE = 512
-GROUPS = 4
+GROUPS = 2
 PIECES = 2
 
 

time: 53 us -> 52.6 us (level)
  no operation moved by 1% of the time
where the time goes in v4:
time: 52.6 us; the launch traced here: 52.5 us
  Pallas kernels  50.8 us (97%)
  local copies, waits for them, and re-layouts  1.67 us (3%)
    pallas_call x1, Pallas kernels, shards(): pl.pallas_call(functools.partial(kernel, S, T), out_shape=jax.ShapeDtypeS...  50.8 us
    unnamed x1, local copies, waits for them, and re-layouts  1.67 us

profile of v4, /device:TPU:0, one launch (start us, length us, event | category | flops | bytes accessed | tf_op | source)
XLA Modules:
  0.0 52.5 jit_solution(11519978235065057433)
XLA Ops:
  0.0 50.8 %shard_map.145 = bf16[64,2048]{1,0:T(8,128)(2,1)} custom-call(bf16[2048]{0:T(1024)(128)(2,1)} %cond_hbm.1, bf16[2048]{0:T(1024)(128)(2,1)} %ctx_cond_hbm.1, f32[1,2048]{1,0:T(1,128)} %bitcast.4, f32[1,2048]{1,0:T(1,128)} %bitcast.5, f32[15,8,31]{2,1,0:T(8,128)} %bitcast.3, bf16[256,2048]{1,0:T(8,128)(2,1)} %latent_hbm.1, bf16[128,2048]{1,0:T(8,128)(2,1)} %context_hbm.1, ...), custom_call_target="tpu_custom_call" | custom-call | tf_op jit(solution)/shard_map/pallas_call | solution.py:759
  50.8 1.7 %copy.17 = bf16[64,2048]{1,0:T(8,128)(2,1)} copy(bf16[64,2048]{1,0:T(8,128)(2,1)} %shard_map.145) | data formatting | bytes 524288
